TPU v7x, 32 devices: a whole 2x2x4 slice. The times are simulated.
32 devices in a mesh: ep: 4 (over y, x), tp: 8 (over z, core).
Axes of the slice: x: 2, y: 2, z: 4, core: 2. Of those that a mesh axis runs over, the one named last changes fastest.
Arguments:
- pool_in: bfloat16 [16384, 1024], P(('ep', 'tp')), may hold values from -6 to 6
- pool_weight: bfloat16 [4, 256, 256], replicated, may hold values from -0.375 to 0.375
- pool_gain: float32 [1024], replicated, may hold values from 0.1 to 1.9
- out_weight: bfloat16 [1024, 2048], P('tp'), may hold values from -0.1875 to 0.1875
- mix_gain: float32 [2048], replicated, may hold values from 0.1 to 1.9
- expert_in: bfloat16 [1024, 2048], P('ep'), may hold values from -6 to 6
- routes: int32 [1024, 4], P('ep'), may hold values from 0 to 7, all different within a row; in each aligned block of 32 rows (0 to 31, 32 to 63, ...) at most 32 rows name the same one
- route_weight: float32 [1024, 4], P('ep'), may hold values from 0.1 to 1
- pre_gain: float32 [2048], replicated, may hold values from 0.1 to 1.9
- gate_weight: bfloat16 [8, 2048, 4096], P('ep', None, 'tp'), may hold values from -0.39648438 to 0.39648438
- up_weight: bfloat16 [8, 2048, 4096], P('ep', None, 'tp'), may hold values from -0.39648438 to 0.39648438
- down_weight: bfloat16 [8, 4096, 2048], P('ep', 'tp'), may hold values from -0.09375 to 0.09375
- post_gain: float32 [2048], replicated, may hold values from 0.1 to 1.9
Outputs:
- mix_out: bfloat16 [16384, 2048], P(('ep', 'tp'))
- expert_out: bfloat16 [1024, 2048], P(('ep', 'tp'))
Inputs may be any that keep to these rules, and one draw needn't show every extreme that they name: `routes`: each row names 4 different experts. In each aligned block of 32 rows no expert is named by more than 32 rows, a bound that some block reaches.
All inputs are finite; a program needn't handle non-finite values.
Results may differ from a plain program's by a relative error of at most 0.019.
Values may be sent and summed in bfloat16 or wider, within the bound.
A program may use at most 128 MiB of HBM per device.

v0:
```python
import jax
import jax.numpy as jnp
from jax import lax
from jax.sharding import PartitionSpec as P

WINDOWS = (2, 4, 8, 16)
EPS = 1e-06
LIMIT = 7.0
ALPHA = 1.702


def shifted(block, axis, distance):
    devices = range(lax.axis_size(axis))
    route = [(i - distance, i) for i in devices if i - distance in devices]
    return lax.ppermute(block, axis, route)


def rms_scale(values, gain):
    mean_square = jnp.mean(values * values, axis=-1, keepdims=True)
    return values * lax.rsqrt(mean_square + EPS) * gain


def trailing_pool(padded, first_pos, rows):
    group = padded.shape[1] // 4
    position = first_pos + jnp.arange(rows, dtype=jnp.int32)
    pieces = []
    for which, window in enumerate(WINDOWS):
        channels = padded[:, which * group : (which + 1) * group]
        running = channels[16 : 16 + rows]
        for reach in range(2, window + 1):
            running = running + channels[17 - reach : 17 - reach + rows]
        count = jnp.minimum(position + 1, window).astype(jnp.float32)[:, None]
        pieces.append(running / count)
    pooled = jnp.concatenate(pieces, axis=1)
    return (pooled - padded[16:]).astype(jnp.bfloat16)


def expert_weights(routes, route_weight, experts):
    chosen = routes[:, :, None] == jnp.arange(experts, dtype=jnp.int32)[None, None, :]
    return jnp.sum(jnp.where(chosen, route_weight[:, :, None], 0.0), axis=1)


def clamped_unit(gate, up):
    gate = jnp.minimum(gate, LIMIT)
    up = jnp.clip(up, -LIMIT, LIMIT)
    return (up + 1.0) * gate * jax.nn.sigmoid(ALPHA * gate)


def body(
    pool_in,
    pool_weight,
    pool_gain,
    out_weight,
    mix_gain,
    expert_in,
    routes,
    route_weight,
    pre_gain,
    gate_weight,
    up_weight,
    down_weight,
    post_gain,
):
    rows, channels = pool_in.shape
    width = out_weight.shape[1]
    rim = shifted(pool_in[rows - 16 :], ("ep", "tp"), 1)
    padded = jnp.concatenate([rim, pool_in], axis=0).astype(jnp.float32)
    first_pos = (lax.axis_index("ep") * lax.axis_size("tp") + lax.axis_index("tp")) * rows
    diff = trailing_pool(padded, first_pos, rows)
    mixed = jnp.einsum(
        "sgc,gcd->sgd",
        diff.reshape(rows, 4, channels // 4),
        pool_weight,
        preferred_element_type=jnp.float32,
    )
    mixed = (mixed.reshape(rows, channels) * pool_gain).astype(jnp.bfloat16)
    projected = jnp.dot(
        mixed,
        lax.all_gather(out_weight, "tp", axis=0, tiled=True),
        preferred_element_type=jnp.float32,
    )
    mix_out = rms_scale(projected, mix_gain).astype(jnp.bfloat16)
    ep_place = lax.axis_index("ep")
    local_experts = gate_weight.shape[0]
    experts = local_experts * lax.axis_size("ep")
    weights = expert_weights(routes, route_weight, experts)
    weights = lax.all_gather(weights, "ep", axis=0, tiled=True)
    weights = lax.dynamic_slice_in_dim(weights, ep_place * local_experts, local_experts, 1)
    normed = rms_scale(expert_in.astype(jnp.float32), pre_gain).astype(jnp.bfloat16)
    normed = lax.all_gather(normed, "ep", axis=0, tiled=True)
    hidden = []
    for which in range(local_experts):
        gate = jnp.dot(normed, gate_weight[which], preferred_element_type=jnp.float32)
        up = jnp.dot(normed, up_weight[which], preferred_element_type=jnp.float32)
        hidden.append((clamped_unit(gate, up) * weights[:, which : which + 1]).astype(jnp.bfloat16))
    hidden = jnp.concatenate(hidden, axis=1)
    partial = jnp.dot(
        hidden, down_weight.reshape(-1, width), preferred_element_type=jnp.float32
    ).astype(jnp.bfloat16)
    combined = lax.psum_scatter(partial, ("ep", "tp"), scatter_dimension=0, tiled=True).astype(
        jnp.float32
    )
    expert_out = rms_scale(combined, post_gain).astype(jnp.bfloat16)
    return (mix_out, expert_out)


def solution(mesh):
    return jax.shard_map(
        body,
        mesh=mesh,
        in_specs=(
            P(("ep", "tp"), None),
            P(),
            P(),
            P("tp", None),
            P(),
            P("ep", None),
            P("ep", None),
            P("ep", None),
            P(),
            P("ep", None, "tp"),
            P("ep", None, "tp"),
            P("ep", "tp", None),
            P(),
        ),
        out_specs=(P(("ep", "tp"), None), P(("ep", "tp"), None)),
        check_vma=False,
    )
```

profile of v0, /device:TPU:0, one launch (start us, length us, event | category | flops | bytes accessed | tf_op | source)
XLA Modules:
  0.0 269.7 jit_solution(13656059231238334772)
XLA Ops:
  7.2 0.0 copy-start
  7.2 0.0 all-gather.5.cloned.1.call-start
  7.2 1.6 fusion
  8.8 0.0 copy-start.5
  8.8 0.0 copy-start.6
  8.8 2.5 fusion.2
  11.3 0.0 all-gather.5.cloned.1.call-update
  11.3 0.0 all-gather.3.cloned.1.call-start
  11.4 0.7 all-gather.3.cloned.1.call-update
  12.1 0.0 reduce-scatter.2.cloned.1.call-start
  12.2 0.0 copy-done.5
  12.2 0.0 copy-done.6
  12.2 9.7 %all_gather.11 = f32[1024,8]{0,1:T(8,128)S(1)} all-gather(f32[256,8]{0,1:T(8,128)S(1)} %select_reduce_fusion), channel_id=1, replica_groups=mesh['ep'=4,'tp'=8] {'ep'}, dimensions={0}, use_global_device_ids=true | all-gather | bytes 40960 | tf_op jit(solution)/shard_map/all_gather | solution.py:87
  21.9 44.9 %all-gather.5.cloned.1.call-done = bf16[1024,2048]{1,0:T(8,128)(2,1)} async-done(((bf16[256,2048]{1,0:T(8,128)(2,1)}), bf16[1024,2048]{1,0:T(8,128)(2,1)}) %all-gather.5.cloned.1.call-update) | async-done | bytes 4194320 | tf_op jit(solution)/shard_map/all_gather | solution.py:90
  66.8 5.4 %fusion.10 = f32[1024,512]{0,1:T(8,128)S(1)} fusion(bf16[1024,2048]{1,0:T(8,128)(2,1)} %all-gather.5.cloned.1.call-done, bf16[2,2048,512]{2,1,0:T(8,128)(2,1)} %param.23), kind=kOutput, calls=%fused_computation.17 | convolution fusion | flops 2147483648 | bytes 8388608 | tf_op jit(solution)/shard_map/dot_general | solution.py:94
  72.2 0.0 copy-done.7
  72.2 0.0 copy-done.10
  72.2 0.0 copy-start.8
  72.2 2.4 fusion.14
  74.6 0.0 copy-done.8
  74.6 3.0 %multiply_convert_fusion.1 = bf16[1024,512]{0,1:T(8,128)(2,1)S(1)} fusion(f32[1024,512]{0,1:T(8,128)S(1)} %fusion.10, bf16[1024,2048]{1,0:T(8,128)(2,1)S(1)} %copy-done.10, bf16[2,2048,512]{2,1,0:T(8,128)(2,1)S(1)} %copy-done.8, f32[1024]{0:T(1024)S(1)} %bitcast.39), kind=kOutput, calls=%fused_computation.23 | convolution fusion | flops 2153250816 | bytes 9441280 | tf_op jit(solution)/shard_map/dot_general | solution.py:93
  77.6 0.0 copy-start.9
  77.7 3.0 %multiply_convert_fusion.2 = bf16[1024,512]{0,1:T(8,128)(2,1)S(1)} fusion(f32[1024,512]{0,1:T(8,128)S(1)} %fusion.14, bf16[1024,2048]{1,0:T(8,128)(2,1)S(1)} %copy-done.10, bf16[2,2048,512]{2,1,0:T(8,128)(2,1)S(1)} %copy-done.8, f32[1024]{0:T(1024)S(1)} %bitcast.38), kind=kOutput, calls=%fused_computation.26 | convolution fusion | flops 2153250816 | bytes 9441280 | tf_op jit(solution)/shard_map/dot_general | solution.py:93
  80.7 0.0 copy-done.9
  80.7 6.5 %convolution_convert_fusion = bf16[1024,2048]{1,0:T(8,128)(2,1)} fusion(bf16[1024,2048]{1,0:T(8,128)(2,1)S(1)} %bitcast.40, bf16[1024,512]{0,1:T(8,128)(2,1)S(1)} %multiply_convert_fusion.1, bf16[1024,512]{0,1:T(8,128)(2,1)S(1)} %multiply_convert_fusion.2), kind=kOutput, calls=%fused_computation.2 | convolution fusion | flops 4301258752 | bytes 10485760 | tf_op jit(solution)/shard_map/dot_general | solution.py:97
  87.1 0.0 reduce-scatter.2.cloned.1.call-update
  87.2 1.2 copy-done.1
  88.4 1.5 collective-permute-start
  90.0 0.8 collective-permute-done
  90.8 0.2 maximum_convert_fusion
  91.0 0.6 fusion.27
  91.7 0.6 fusion.30
  92.3 0.4 fusion.3
  92.7 0.0 copy-start.4
  92.8 0.0 copy-done
  92.8 0.5 fusion.24
  93.3 0.2 copy-done.4
  93.4 0.2 fusion.7
  93.6 0.0 copy-start.2
  93.7 22.0 %all-gather.3.cloned.1.call-done = bf16[1024,2048]{1,0:T(8,128)(2,1)} async-done(((bf16[128,2048]{1,0:T(8,128)(2,1)}), bf16[1024,2048]{1,0:T(8,128)(2,1)}) %all-gather.3.cloned.1.call-update) | async-done | bytes 4194320 | tf_op jit(solution)/shard_map/all_gather | solution.py:79
  115.6 4.7 %multiply_reduce_fusion = (f32[512]{0:T(512)S(1)}, f32[512,2048]{1,0:T(8,128)S(1)}) fusion(bf16[512,1024]{0,1:T(8,128)(2,1)S(1)} %fusion.7, bf16[1024,2048]{1,0:T(8,128)(2,1)} %all-gather.3.cloned.1.call-done), kind=kOutput, calls=%fused_computation.1 | convolution fusion | flops 2149580288 | bytes 9439232 | tf_op jit(solution)/shard_map/dot_general | solution.py:77
  120.3 0.0 copy-done.2
  120.3 0.0 copy-start.3
  120.3 1.7 multiply_convert_fusion
  122.1 138.4 %reduce-scatter.2.cloned.1.call-done = bf16[32,2048]{1,0:T(8,128)(2,1)} async-done(((bf16[1024,2048]{1,0:T(8,128)(2,1)}), bf16[32,2048]{1,0:T(8,128)(2,1)}) %reduce-scatter.2.cloned.1.call-update) | async-done | bytes 131088 | tf_op jit(solution)/shard_map/reduce_scatter | solution.py:100
  260.5 1.0 fusion.31
  261.5 0.0 copy-done.3
  261.6 1.7 fusion.33
  (11 shorter events, 0.1 us)
Async XLA Ops:
  7.2 85.6 %copy-start = (bf16[4,256,256]{2,1,0:T(8,128)(2,1)S(1)}, bf16[4,256,256]{2,1,0:T(8,128)(2,1)}, u32[]{:S(2)}) copy-start(bf16[4,256,256]{2,1,0:T(8,128)(2,1)} %param.14) | copy-start | bytes 1572868
  7.2 59.6 %all-gather.5.cloned.1.call-start = ((), (), s32[]{:S(2)}) async-start(), calls=%async_computation.2 | async-start | bytes 5242880 | tf_op jit(solution)/shard_map/all_gather | solution.py:90
  8.8 3.4 %copy-start.5 = (f32[256,4]{0,1:T(4,128)S(1)}, f32[256,4]{0,1:T(4,128)}, u32[]{:S(2)}) copy-start(f32[256,4]{0,1:T(4,128)} %param.20) | copy-start | bytes 12292
  8.8 3.4 %copy-start.6 = (s32[256,4]{0,1:T(4,128)S(1)}, s32[256,4]{0,1:T(4,128)}, u32[]{:S(2)}) copy-start(s32[256,4]{0,1:T(4,128)} %param.19) | copy-start | bytes 12292
  11.3 104.3 %all-gather.3.cloned.1.call-start = ((), (), s32[]{:S(2)}) async-start(), calls=%async_computation.1 | async-start | bytes 4718592 | tf_op jit(solution)/shard_map/all_gather | solution.py:79
  12.1 248.4 %reduce-scatter.2.cloned.1.call-start = ((), (), s32[]{:S(2)}) async-start(), calls=%async_computation.3 | async-start | bytes 4325376 | tf_op jit(solution)/shard_map/reduce_scatter | solution.py:100
  66.8 5.4 %copy-start.7 = (bf16[2,2048,512]{2,1,0:T(8,128)(2,1)S(1)}, bf16[2,2048,512]{2,1,0:T(8,128)(2,1)}, u32[]{:S(2)}) copy-start(bf16[2,2048,512]{2,1,0:T(8,128)(2,1)} %param.23) | copy-start | bytes 12582916
  66.8 5.4 %copy-start.10 = (bf16[1024,2048]{1,0:T(8,128)(2,1)S(1)}, bf16[1024,2048]{1,0:T(8,128)(2,1)}, u32[]{:S(2)}) copy-start(bf16[1024,2048]{1,0:T(8,128)(2,1)} %all-gather.5.cloned.1.call-done) | copy-start | bytes 12582916
  72.2 2.4 copy-start.8
  77.6 3.0 %copy-start.9 = (bf16[2,512,2048]{2,1,0:T(8,128)(2,1)S(1)}, bf16[2,512,2048]{2,1,0:T(8,128)(2,1)}, u32[]{:S(2)}) copy-start(bf16[2,512,2048]{2,1,0:T(8,128)(2,1)} %param.24) | copy-start | bytes 12582916
  87.1 1.3 copy-start.1
  88.4 2.4 collective-permute-start
  92.7 0.7 copy-start.4
  93.6 26.7 %copy-start.2 = (f32[2048]{0:T(1024)S(1)}, f32[2048]{0:T(1024)}, u32[]{:S(2)}) copy-start(f32[2048]{0:T(1024)} %param.17) | copy-start | bytes 24580
  120.3 141.2 %copy-start.3 = (f32[2048]{0:T(1024)S(1)}, f32[2048]{0:T(1024)}, u32[]{:S(2)}) copy-start(f32[2048]{0:T(1024)} %param.25) | copy-start | bytes 24580
Sparse Core Ops, SparseCore 0:
  11.5 55.2 all-gather.4
  68.4 47.2 all-gather.2
  117.9 142.5 reduce-scatter.1
where the time goes:
time: 270 us
  waiting for transfers between devices  207 us (77%)
  matrix products  25.4 us (9%)
  between operations  14 us (5%)
  other arithmetic  10.7 us (4%)
  blocking collectives  9.67 us (4%)
    reduce_scatter x1, waiting for transfers between devices, body(): lax.psum_scatter(partial, ('ep', 'tp'), scatter_dimension=0, tiled=True)  138 us
    all_gather x1, waiting for transfers between devices, body(): normed = lax.all_gather(normed, 'ep', axis=0, tiled=True)  44.9 us
    all_gather x1, waiting for transfers between devices, body(): lax.all_gather(out_weight, 'tp', axis=0, tiled=True)  22 us
    all_gather x1, blocking collectives, body(): weights = lax.all_gather(weights, 'ep', axis=0, tiled=True)  9.67 us
    dot_general x2, matrix products, body(): up = jnp.dot(normed, up_weight[which], preferred_element_type=jnp.float32)  7.79 us
    dot_general x1, matrix products, body(): jnp.dot(hidden, down_weight.reshape(-1, width), preferred_element_type=jn...  6.47 us
    dot_general x2, matrix products, body(): jnp.dot(normed, gate_weight[which], preferred_element_type=jnp.float32)  5.99 us
  transfers between devices with their start and end apart: 4, of which 4 were waited for; matrix products, arithmetic and copies ran while one was open for 11% of the time, Pallas kernels for 0%

commit v1 on v0

--- a/solution.py
+++ b/solution.py
@@ -76,7 +76,9 @@
     mixed = (mixed.reshape(rows, channels) * pool_gain).astype(jnp.bfloat16)
     projected = jnp.dot(
         mixed,
-        lax.all_gather(out_weight, "tp", axis=0, tiled=True),
+        jnp.concatenate(
+            lax.all_to_all(jnp.stack([out_weight] * lax.axis_size("tp")), "tp", 0, 0), axis=0
+        ),
         preferred_element_type=jnp.float32,
     )
     mix_out = rms_scale(projected, mix_gain).astype(jnp.bfloat16)

time: 270 us -> 242 us (0.90)
  waiting for transfers between devices: 207 us -> 171 us
  starting transfers between devices: 1.64 us -> 8.12 us
    reduce_scatter x1, waiting for transfers between devices: 138 us -> 99.1 us  [body(): lax.psum_scatter(partial, ('ep', 'tp'), scatter_dimension=0, tiled=True)]
    all_to_all x0 -> x1, waiting for transfers between devices: none -> 33.3 us  [body(): lax.all_to_all(jnp.stack([out_weight] * lax.axis_size('tp')), 'tp', 0, 0)]
    all_gather x1 -> x0, waiting for transfers between devices: 22 us -> none  [body(): lax.all_gather(out_weight, 'tp', axis=0, tiled=True)]
    all_gather x1, waiting for transfers between devices: 44.9 us -> 37.9 us  [body(): normed = lax.all_gather(normed, 'ep', axis=0, tiled=True)]
    all_to_all x0 -> x1, starting transfers between devices: none -> 6.49 us  [body(): lax.all_to_all(jnp.stack([out_weight] * lax.axis_size('tp')), 'tp', 0, 0)]
  transfers between devices with their start and end apart: 4 -> 4, of which waited for: 4 -> 4; matrix products, arithmetic and copies ran while one was open for 11% -> 13% of each run, Pallas kernels for 0% -> 0%
where the time goes in v1:
time: 242 us
  waiting for transfers between devices  171 us (71%)
  matrix products  25.4 us (10%)
  between operations  14.3 us (6%)
  other arithmetic  10.5 us (4%)
  blocking collectives  8.7 us (4%)
  starting transfers between devices  8.12 us (3%)
  local copies, waits for them, and re-layouts  3.79 us (2%)
    reduce_scatter x1, waiting for transfers between devices, body(): lax.psum_scatter(partial, ('ep', 'tp'), scatter_dimension=0, tiled=True)  99.1 us
    all_gather x1, waiting for transfers between devices, body(): normed = lax.all_gather(normed, 'ep', axis=0, tiled=True)  37.9 us
    all_to_all x1, waiting for transfers between devices, body(): lax.all_to_all(jnp.stack([out_weight] * lax.axis_size('tp')), 'tp', 0, 0)  33.3 us
    all_gather x1, blocking collectives, body(): weights = lax.all_gather(weights, 'ep', axis=0, tiled=True)  8.7 us
    dot_general x2, matrix products, body(): up = jnp.dot(normed, up_weight[which], preferred_element_type=jnp.float32)  7.78 us
    all_to_all x1, starting transfers between devices, body(): lax.all_to_all(jnp.stack([out_weight] * lax.axis_size('tp')), 'tp', 0, 0)  6.49 us
    dot_general x1, matrix products, body(): jnp.dot(hidden, down_weight.reshape(-1, width), preferred_element_type=jn...  6.45 us
    dot_general x2, matrix products, body(): jnp.dot(normed, gate_weight[which], preferred_element_type=jnp.float32)  5.99 us
  transfers between devices with their start and end apart: 4, of which 4 were waited for; matrix products, arithmetic and copies ran while one was open for 13% of the time, Pallas kernels for 0%

profile of v1, /device:TPU:0, one launch (start us, length us, event | category | flops | bytes accessed | tf_op | source)
XLA Modules:
  0.0 241.8 jit_solution(7534253019966431960)
XLA Ops:
  7.2 0.0 copy-start
  7.2 0.0 copy-start.2
  7.2 0.0 all-gather.2.cloned.1.call-start
  7.2 1.6 fusion
  8.8 2.5 %fusion.2 = bf16[256,2048]{1,0:T(8,128)(2,1)} fusion(bf16[256,2048]{1,0:T(8,128)(2,1)} %param.18, f32[2048]{0:T(1024)} %param.21, f32[256]{0:T(256)S(1)} %add_rsqrt_fusion.1), kind=kLoop, calls=%fused_computation.7 | loop fusion | flops 2097152 | bytes 2106368 | tf_op jit(solution)/shard_map/convert_element_type | solution.py:91
  11.4 0.0 all-gather.2.cloned.1.call-update
  11.4 0.0 copy-done.2
  11.4 2.5 %stack.2 = bf16[8,128,2048]{2,1,0:T(8,128)(2,1)} broadcast(bf16[128,2048]{1,0:T(8,128)(2,1)S(1)} %copy-done.2), dimensions={1,2} | broadcast | bytes 4718592 | tf_op jit(solution)/shard_map/stack | solution.py:80
  13.9 0.0 copy-start.6
  13.9 0.0 copy-start.7
  13.9 6.5 %all-to-all-start = ((bf16[8,128,2048]{2,1,0:T(8,128)(2,1)}), bf16[8,128,2048]{2,1,0:T(8,128)(2,1)}, u32[]{:S(2)}, u32[]{:S(2)}) async-start(bf16[8,128,2048]{2,1,0:T(8,128)(2,1)} %stack.2), calls=%async_computation | async-start | bytes 8388608 | tf_op jit(solution)/shard_map/all_to_all | solution.py:80
  20.4 0.0 reduce-scatter.2.cloned.1.call-start
  20.5 0.0 copy-done.6
  20.5 0.0 copy-done.7
  20.5 8.7 %all_gather.7 = f32[1024,8]{0,1:T(8,128)S(1)} all-gather(f32[256,8]{0,1:T(8,128)S(1)} %select_reduce_fusion), channel_id=1, replica_groups=mesh['ep'=4,'tp'=8] {'ep'}, dimensions={0}, use_global_device_ids=true | all-gather | bytes 40960 | tf_op jit(solution)/shard_map/all_gather | solution.py:89
  29.2 37.9 %all-gather.2.cloned.1.call-done = bf16[1024,2048]{1,0:T(8,128)(2,1)} async-done(((bf16[256,2048]{1,0:T(8,128)(2,1)}), bf16[1024,2048]{1,0:T(8,128)(2,1)}) %all-gather.2.cloned.1.call-update) | async-done | bytes 4194320 | tf_op jit(solution)/shard_map/all_gather | solution.py:92
  67.1 0.0 copy-start.8
  67.1 5.4 %fusion.9 = f32[1024,512]{0,1:T(8,128)S(1)} fusion(bf16[1024,2048]{1,0:T(8,128)(2,1)} %all-gather.2.cloned.1.call-done, bf16[2,2048,512]{2,1,0:T(8,128)(2,1)} %param.23), kind=kOutput, calls=%fused_computation.15 | convolution fusion | flops 2147483648 | bytes 8388608 | tf_op jit(solution)/shard_map/dot_general | solution.py:96
  72.5 0.0 copy-done.8
  72.5 0.0 copy-done.11
  72.5 0.0 copy-start.9
  72.5 2.4 fusion.13
  74.9 0.0 copy-done.9
  74.9 3.0 %multiply_convert_fusion.1 = bf16[1024,512]{0,1:T(8,128)(2,1)S(1)} fusion(f32[1024,512]{0,1:T(8,128)S(1)} %fusion.9, bf16[1024,2048]{1,0:T(8,128)(2,1)S(1)} %copy-done.11, bf16[2,2048,512]{2,1,0:T(8,128)(2,1)S(1)} %copy-done.9, f32[1024]{0:T(1024)S(1)} %bitcast.38), kind=kOutput, calls=%fused_computation.21 | convolution fusion | flops 2153250816 | bytes 9441280 | tf_op jit(solution)/shard_map/dot_general | solution.py:95
  77.9 0.0 copy-start.10
  77.9 3.0 %multiply_convert_fusion.2 = bf16[1024,512]{0,1:T(8,128)(2,1)S(1)} fusion(f32[1024,512]{0,1:T(8,128)S(1)} %fusion.13, bf16[1024,2048]{1,0:T(8,128)(2,1)S(1)} %copy-done.11, bf16[2,2048,512]{2,1,0:T(8,128)(2,1)S(1)} %copy-done.9, f32[1024]{0:T(1024)S(1)} %bitcast.37), kind=kOutput, calls=%fused_computation.24 | convolution fusion | flops 2153250816 | bytes 9441280 | tf_op jit(solution)/shard_map/dot_general | solution.py:95
  80.9 0.0 copy-done.10
  81.0 6.5 %convolution_convert_fusion = bf16[1024,2048]{1,0:T(8,128)(2,1)} fusion(bf16[1024,2048]{1,0:T(8,128)(2,1)S(1)} %bitcast.39, bf16[1024,512]{0,1:T(8,128)(2,1)S(1)} %multiply_convert_fusion.1, bf16[1024,512]{0,1:T(8,128)(2,1)S(1)} %multiply_convert_fusion.2), kind=kOutput, calls=%fused_computation.2 | convolution fusion | flops 4301258752 | bytes 10485760 | tf_op jit(solution)/shard_map/dot_general | solution.py:99
  87.4 0.0 reduce-scatter.2.cloned.1.call-update
  87.4 1.2 copy-done.1
  88.6 1.6 collective-permute-start
  90.2 0.0 copy-done.5
  90.3 0.8 collective-permute-done
  91.0 0.2 maximum_convert_fusion
  91.3 0.6 fusion.25
  91.9 0.6 fusion.28
  92.6 0.4 fusion.3
  93.0 0.0 copy-done
  93.0 0.5 multiply_convert_fusion.3
  93.5 33.3 %all-to-all-done = bf16[8,128,2048]{2,1,0:T(8,128)(2,1)} async-done(((bf16[8,128,2048]{2,1,0:T(8,128)(2,1)}), bf16[8,128,2048]{2,1,0:T(8,128)(2,1)}, u32[]{:S(2)}, u32[]{:S(2)}) %all-to-all-start) | async-done | bytes 4194336 | tf_op jit(solution)/shard_map/all_to_all | solution.py:80
  126.8 4.7 %multiply_reduce_fusion = (f32[512]{0:T(512)S(1)}, f32[512,2048]{1,0:T(8,128)S(1)}) fusion(bf16[512,1024]{0,1:T(8,128)(2,1)S(1)} %bitcast.35, bf16[1024,2048]{1,0:T(8,128)(2,1)} %bitcast.2), kind=kOutput, calls=%fused_computation.1 | convolution fusion | flops 2149580288 | bytes 9439232 | tf_op jit(solution)/shard_map/dot_general | solution.py:77
  131.5 0.0 copy-done.3
  131.5 0.0 copy-start.4
  131.5 1.7 multiply_convert_fusion
  133.2 99.1 %reduce-scatter.2.cloned.1.call-done = bf16[32,2048]{1,0:T(8,128)(2,1)} async-done(((bf16[1024,2048]{1,0:T(8,128)(2,1)}), bf16[32,2048]{1,0:T(8,128)(2,1)}) %reduce-scatter.2.cloned.1.call-update) | async-done | bytes 131088 | tf_op jit(solution)/shard_map/reduce_scatter | solution.py:102
  232.3 1.0 fusion.29
  233.3 0.0 copy-done.4
  233.3 1.7 fusion.31
  (13 shorter events, 0.1 us)
Async XLA Ops:
  7.2 85.8 %copy-start = (bf16[4,256,256]{2,1,0:T(8,128)(2,1)S(1)}, bf16[4,256,256]{2,1,0:T(8,128)(2,1)}, u32[]{:S(2)}) copy-start(bf16[4,256,256]{2,1,0:T(8,128)(2,1)} %param.14) | copy-start | bytes 1572868
  7.2 4.2 %copy-start.2 = (bf16[128,2048]{1,0:T(8,128)(2,1)S(1)}, bf16[128,2048]{1,0:T(8,128)(2,1)}, u32[]{:S(2)}) copy-start(bf16[128,2048]{1,0:T(8,128)(2,1)} %param.16) | copy-start | bytes 1572868
  7.2 59.9 %all-gather.2.cloned.1.call-start = ((), (), s32[]{:S(2)}) async-start(), calls=%async_computation.2 | async-start | bytes 5242880 | tf_op jit(solution)/shard_map/all_gather | solution.py:92
  13.9 6.5 %copy-start.6 = (f32[256,4]{0,1:T(4,128)S(1)}, f32[256,4]{0,1:T(4,128)}, u32[]{:S(2)}) copy-start(f32[256,4]{0,1:T(4,128)} %param.20) | copy-start | bytes 12292
  13.9 6.6 %copy-start.7 = (s32[256,4]{0,1:T(4,128)S(1)}, s32[256,4]{0,1:T(4,128)}, u32[]{:S(2)}) copy-start(s32[256,4]{0,1:T(4,128)} %param.19) | copy-start | bytes 12292
  13.9 112.9 %all-to-all-start = ((bf16[8,128,2048]{2,1,0:T(8,128)(2,1)}), bf16[8,128,2048]{2,1,0:T(8,128)(2,1)}, u32[]{:S(2)}, u32[]{:S(2)}) async-start(bf16[8,128,2048]{2,1,0:T(8,128)(2,1)} %stack.2), calls=%async_computation | async-start | bytes 8388608 | tf_op jit(solution)/shard_map/all_to_all | solution.py:80
  20.4 211.9 %reduce-scatter.2.cloned.1.call-start = ((), (), s32[]{:S(2)}) async-start(), calls=%async_computation.3 | async-start | bytes 4325376 | tf_op jit(solution)/shard_map/reduce_scatter | solution.py:102
  67.1 5.4 %copy-start.8 = (bf16[2,2048,512]{2,1,0:T(8,128)(2,1)S(1)}, bf16[2,2048,512]{2,1,0:T(8,128)(2,1)}, u32[]{:S(2)}) copy-start(bf16[2,2048,512]{2,1,0:T(8,128)(2,1)} %param.23) | copy-start | bytes 12582916
  67.1 5.4 %copy-start.11 = (bf16[1024,2048]{1,0:T(8,128)(2,1)S(1)}, bf16[1024,2048]{1,0:T(8,128)(2,1)}, u32[]{:S(2)}) copy-start(bf16[1024,2048]{1,0:T(8,128)(2,1)} %all-gather.2.cloned.1.call-done) | copy-start | bytes 12582916
  72.5 2.4 %copy-start.9 = (bf16[2,2048,512]{2,1,0:T(8,128)(2,1)S(1)}, bf16[2,2048,512]{2,1,0:T(8,128)(2,1)}, u32[]{:S(2)}) copy-start(bf16[2,2048,512]{2,1,0:T(8,128)(2,1)} %param.22) | copy-start | bytes 12582916
  77.9 3.0 %copy-start.10 = (bf16[2,512,2048]{2,1,0:T(8,128)(2,1)S(1)}, bf16[2,512,2048]{2,1,0:T(8,128)(2,1)}, u32[]{:S(2)}) copy-start(bf16[2,512,2048]{2,1,0:T(8,128)(2,1)} %param.24) | copy-start | bytes 12582916
  87.4 1.2 copy-start.1
  87.4 2.8 %copy-start.5 = (f32[1024]{0:T(1024)S(1)}, f32[1024]{0:T(1024)}, u32[]{:S(2)}) copy-start(f32[1024]{0:T(1024)} %param.15) | copy-start | bytes 12292
  88.6 2.4 collective-permute-start
  126.8 4.7 %copy-start.3 = (f32[2048]{0:T(1024)S(1)}, f32[2048]{0:T(1024)}, u32[]{:S(2)}) copy-start(f32[2048]{0:T(1024)} %param.17) | copy-start | bytes 24580
  131.5 101.9 %copy-start.4 = (f32[2048]{0:T(1024)S(1)}, f32[2048]{0:T(1024)}, u32[]{:S(2)}) copy-start(f32[2048]{0:T(1024)} %param.25) | copy-start | bytes 24580
Sparse Core Ops, SparseCore 0:
  11.5 55.5 all-gather.1
  87.6 144.6 reduce-scatter.1
